TPU v7x, 32 devices: a whole 2x2x4 slice. The times are simulated.
32 devices in a mesh: rep: 2 (over x), fs: 8 (over z, y), tp: 2 (over core).
Axes of the slice: x: 2, y: 2, z: 4, core: 2. Of those that a mesh axis runs over, the one named last changes fastest.
Arguments:
- residual: bfloat16 [16, 384, 2048], P(('rep', 'fs'), None, 'tp'), may hold values from -6 to 6
- gain_first: float32 [2048], replicated, may hold values from 0.1 to 1.9
- gain_mixer: float32 [2048], replicated, may hold values from 0.1 to 1.9
- gain_last: float32 [2048], replicated, may hold values from 0.1 to 1.9
- hidden_gate: float32 [2048, 6144], P('fs', 'tp'), may hold values from -0.125 to 0.125
- hidden_up: float32 [2048, 6144], P('fs', 'tp'), may hold values from -0.125 to 0.125
- hidden_down: float32 [6144, 2048], P('tp', 'fs'), may hold values from -0.078125 to 0.078125
- gate_scale: float32 [6144], replicated, may hold values from 0.5 to 2
- up_scale: float32 [6144], replicated, may hold values from 0.5 to 2
- down_scale: float32 [2048], replicated, may hold values from 0.5 to 2
- mix_value: float32 [2048, 2048], P('fs', 'tp'), may hold values from -0.125 to 0.125
- mix_gate: float32 [2048, 2048], P('fs', 'tp'), may hold values from -0.125 to 0.125
- value_scale: float32 [2048], replicated, may hold values from 0.5 to 2
- gating_scale: float32 [2048], replicated, may hold values from 0.5 to 2
- mix_taps: float32 [31, 2048], replicated, may hold values from -1.25 to 1.25
- mix_gain: float32 [2048], replicated, may hold values from 0.1 to 1.9
- mix_out: float32 [2048, 2048], P('tp', 'fs'), may hold values from -0.125 to 0.125
- out_scale: float32 [2048], replicated, may hold values from 0.5 to 2
Outputs:
- updated: bfloat16 [16, 384, 2048], P(('rep', 'fs'), None, 'tp')
All inputs are finite; a program needn't handle non-finite values.
Results may differ from a plain program's by a relative error of at most 0.024.
Values may be sent and summed in bfloat16 or wider, within the bound.
A program may use at most 128 MiB of HBM per device.

v0:
```python
import jax
import jax.numpy as jnp
from jax import lax
from jax.sharding import PartitionSpec as P

EPS = 1e-06


def fold_rows(normed, pieces):
    return (
        jnp.dot(normed, pieces[0], preferred_element_type=jnp.float32),
        jnp.dot(normed, pieces[1], preferred_element_type=jnp.float32),
    )


def column_product(left, scale, piece):
    return jnp.dot(left, piece, preferred_element_type=jnp.float32) * scale


def on_device(
    residual,
    gain_first,
    gain_mixer,
    gain_last,
    hidden_gate,
    hidden_up,
    hidden_down,
    gate_scale,
    up_scale,
    down_scale,
    mix_value,
    mix_gate,
    value_scale,
    gating_scale,
    mix_taps,
    mix_gain,
    mix_out,
    out_scale,
):
    tp_rank = lax.axis_index("tp")
    hidden_local = hidden_gate.shape[1]
    width_local = residual.shape[2]
    seq_len = residual.shape[1]
    gate_cols = lax.dynamic_slice_in_dim(gate_scale, tp_rank * hidden_local, hidden_local)
    up_cols = lax.dynamic_slice_in_dim(up_scale, tp_rank * hidden_local, hidden_local)
    value_cols = lax.dynamic_slice_in_dim(value_scale, tp_rank * width_local, width_local)
    gating_cols = lax.dynamic_slice_in_dim(gating_scale, tp_rank * width_local, width_local)
    gain_cols = lax.dynamic_slice_in_dim(mix_gain, tp_rank * width_local, width_local)
    tap_cols = lax.dynamic_slice_in_dim(mix_taps, tp_rank * width_local, width_local, 1)
    gate_half = hidden_gate.astype(jnp.bfloat16)
    up_half = hidden_up.astype(jnp.bfloat16)
    down_half = hidden_down.astype(jnp.bfloat16)
    value_half = mix_value.astype(jnp.bfloat16)
    mgate_half = mix_gate.astype(jnp.bfloat16)
    out_half = mix_out.astype(jnp.bfloat16)

    def normed_rows(stream, gain):
        gathered = lax.all_gather(stream, "tp", axis=1, tiled=True)
        values = gathered.astype(jnp.float32)
        scaled = values * lax.rsqrt(jnp.mean(values * values, axis=-1, keepdims=True) + EPS) * gain
        return scaled.astype(jnp.bfloat16)

    def spread_sum(terms):
        return lax.psum_scatter(
            terms.astype(jnp.bfloat16), "tp", scatter_dimension=1, tiled=True
        ).astype(jnp.float32)

    def inner_half(stream, gain):
        normed = normed_rows(stream, gain)
        gate, upward = fold_rows(
            normed,
            (
                lax.all_gather(gate_half, "fs", axis=0, tiled=True),
                lax.all_gather(up_half, "fs", axis=0, tiled=True),
            ),
        )
        hidden = (jax.nn.silu(gate * gate_cols) * (upward * up_cols)).astype(jnp.bfloat16)
        terms = column_product(
            hidden, down_scale, lax.all_gather(down_half, "fs", axis=1, tiled=True)
        )
        return spread_sum(terms)

    stream = residual[0]
    first = (stream.astype(jnp.float32) + 0.5 * inner_half(stream, gain_first)).astype(jnp.bfloat16)
    normed = normed_rows(first, gain_mixer)
    value, gating = fold_rows(
        normed,
        (
            lax.all_gather(value_half, "fs", axis=0, tiled=True),
            lax.all_gather(mgate_half, "fs", axis=0, tiled=True),
        ),
    )
    glu = lax.optimization_barrier(
        (value * value_cols * jax.nn.sigmoid(gating * gating_cols)).astype(jnp.bfloat16)
    ).astype(jnp.float32)
    span = tap_cols.shape[0]
    padded = jnp.pad(glu, ((span - 1, 0), (0, 0)))
    wave = jnp.zeros_like(glu)
    for offset in range(span):
        wave = wave + tap_cols[offset] * padded[span - 1 - offset : span - 1 - offset + seq_len]
    total_sq = lax.psum(jnp.sum(wave * wave, axis=1), "tp")
    inverse = lax.rsqrt(total_sq / mix_taps.shape[1] + EPS)
    acted = jax.nn.silu(wave * inverse[:, None] * gain_cols).astype(jnp.bfloat16)
    terms = column_product(acted, out_scale, lax.all_gather(out_half, "fs", axis=1, tiled=True))
    second = (first.astype(jnp.float32) + spread_sum(terms)).astype(jnp.bfloat16)
    updated = (second.astype(jnp.float32) + 0.5 * inner_half(second, gain_last)).astype(
        jnp.bfloat16
    )
    return updated[None]


def solution(mesh):
    in_specs = (
        P(("rep", "fs"), None, "tp"),
        P(),
        P(),
        P(),
        P("fs", "tp"),
        P("fs", "tp"),
        P("tp", "fs"),
        P(),
        P(),
        P(),
        P("fs", "tp"),
        P("fs", "tp"),
        P(),
        P(),
        P(),
        P(),
        P("tp", "fs"),
        P(),
    )
    out_specs = P(("rep", "fs"), None, "tp")
    return jax.shard_map(
        on_device, mesh=mesh, in_specs=in_specs, out_specs=out_specs, check_vma=False
    )
```

profile of v0, /device:TPU:0, one launch (start us, length us, event | category | flops | bytes accessed | tf_op | source)
XLA Modules:
  0.0 900.1 jit_solution(637089719911600828)
XLA Ops:
  6.5 0.7 all-gather.27.cloned.1.call-update
  7.3 3.4 convert_element_type.92
  10.7 0.0 all-gather.13.cloned.1.call-start
  10.8 1.4 convert_element_type.93
  12.3 0.0 all-gather.15.cloned.1.call-start
  12.3 3.2 convert_element_type.95
  15.5 0.0 reduce-scatter.4.cloned.1.call-start
  15.6 0.7 copy-done.10
  16.3 5.2 all-gather.27.cloned.1.call-done
  21.4 1.9 fusion.6
  23.4 177.6 %all-gather.11.cloned.1.call-done = bf16[2048,3072]{1,0:T(8,128)(2,1)} async-done(((bf16[256,3072]{1,0:T(8,128)(2,1)}), bf16[2048,3072]{1,0:T(8,128)(2,1)}) %all-gather.11.cloned.1.call-update) | async-done | bytes 12582928 | tf_op jit(solution)/shard_map/all_gather | solution.py:73
  200.9 10.3 %fusion.22 = f32[384,3072]{1,0:T(8,128)} fusion(bf16[2048,3072]{1,0:T(8,128)(2,1)} %all-gather.11.cloned.1.call-done, bf16[1,384,2048]{2,1,0:T(8,128)(2,1)S(1)} %copy-done.5, f32[2048]{0:T(1024)S(1)} %copy-done.12, f32[384]{0:T(512)S(1)} %add_rsqrt_fusion.3), kind=kOutput, calls=%fused_computation.41 | convolution fusion | flops 4834983936 | bytes 18884096 | tf_op jit(solution)/shard_map/dot_general | solution.py:11
  211.3 166.2 %all-gather.13.cloned.1.call-done = bf16[2048,3072]{1,0:T(8,128)(2,1)} async-done(((bf16[256,3072]{1,0:T(8,128)(2,1)}), bf16[2048,3072]{1,0:T(8,128)(2,1)}) %all-gather.13.cloned.1.call-update) | async-done | bytes 12582928 | tf_op jit(solution)/shard_map/all_gather | solution.py:74
  377.4 176.2 %all-gather.15.cloned.1.call-done = bf16[3072,2048]{1,0:T(8,128)(2,1)} async-done(((bf16[3072,256]{1,0:T(8,128)(2,1)}), bf16[3072,2048]{1,0:T(8,128)(2,1)}) %all-gather.15.cloned.1.call-update) | async-done | bytes 12582928 | tf_op jit(solution)/shard_map/all_gather | solution.py:79
  553.7 21.3 %multiply_convert_fusion.4 = bf16[384,2048]{1,0:T(8,128)(2,1)} fusion(bf16[3072,2048]{1,0:T(8,128)(2,1)} %all-gather.15.cloned.1.call-done, f32[2048]{0:T(1024)S(1)} %copy-done.15, f32[384,3072]{1,0:T(8,128)} %fusion.22, bf16[2048,3072]{1,0:T(8,128)(2,1)} %all-gather.13.cloned.1.call-done, f32[3072]{0:T(1024)S(1)} %dynamic_slice.19, ...), kind=kOutput, calls=%fused_computation.19 | convolution fusion | flops 9677832192 | bytes 33072640 | tf_op jit(solution)/shard_map/dot_general | solution.py:17
  575.0 0.0 all-gather.17.cloned.1.call-start
  575.1 7.2 reduce-scatter.4.cloned.1.call-done
  582.3 2.3 fusion.9
  584.6 0.0 all-gather.19.cloned.1.call-start
  584.7 0.9 convert_element_type.102
  585.6 0.2 all-gather.21.cloned.1.call-start
  585.8 0.2 copy-done.8
  586.0 0.9 convert_element_type.103
  586.9 0.0 all-gather.23.cloned.1.call-start
  586.9 0.9 convert_element_type.107
  587.8 0.0 reduce-scatter.6.cloned.1.call-start
  587.9 1.3 fusion.34
  589.2 1.6 constant_dynamic-slice_fusion
  590.8 5.1 all-gather.17.cloned.1.call-done
  595.8 1.9 fusion
  597.8 74.2 %all-gather.19.cloned.1.call-done = bf16[2048,1024]{1,0:T(8,128)(2,1)} async-done(((bf16[256,1024]{1,0:T(8,128)(2,1)}), bf16[2048,1024]{1,0:T(8,128)(2,1)}) %all-gather.19.cloned.1.call-update) | async-done | bytes 4194320 | tf_op jit(solution)/shard_map/all_gather | solution.py:89
  672.0 5.2 fusion.29
  677.2 68.3 %all-gather.21.cloned.1.call-done = bf16[2048,1024]{1,0:T(8,128)(2,1)} async-done(((bf16[256,1024]{1,0:T(8,128)(2,1)}), bf16[2048,1024]{1,0:T(8,128)(2,1)}) %all-gather.21.cloned.1.call-update) | async-done | bytes 4194320 | tf_op jit(solution)/shard_map/all_gather | solution.py:90
  745.4 4.7 multiply_convert_fusion.6
  750.2 0.2 convert_element_type.105
  750.4 7.3 multiply_reduce_fusion
  757.7 2.5 psum.7
  760.1 60.6 %all-gather.23.cloned.1.call-done = bf16[1024,2048]{1,0:T(8,128)(2,1)} async-done(((bf16[1024,256]{1,0:T(8,128)(2,1)}), bf16[1024,2048]{1,0:T(8,128)(2,1)}) %all-gather.23.cloned.1.call-update) | async-done | bytes 4194320 | tf_op jit(solution)/shard_map/all_gather | solution.py:104
  820.7 5.5 multiply_convert_fusion.3
  826.3 7.2 reduce-scatter.6.cloned.1.call-done
  833.5 2.3 add_convert_fusion.1
  835.9 0.3 reduce-scatter.8.cloned.1.call-start
  836.1 11.0 %all-gather.25.cloned.1.call-done = bf16[384,2048]{1,0:T(8,128)(2,1)} async-done(((bf16[384,1024]{1,0:T(8,128)(2,1)}), bf16[384,2048]{1,0:T(8,128)(2,1)}) %all-gather.25.cloned.1.call-update) | async-done | bytes 1572880 | tf_op jit(solution)/shard_map/all_gather | solution.py:58
  847.1 1.9 fusion.3
  849.0 10.3 %fusion.26 = f32[384,3072]{1,0:T(8,128)} fusion(bf16[2048,3072]{1,0:T(8,128)(2,1)} %all-gather.11.cloned.1.call-done, bf16[384,2048]{1,0:T(8,128)(2,1)S(1)} %copy-done.6, f32[2048]{0:T(1024)S(1)} %copy-done.16, f32[384]{0:T(512)S(1)} %add_rsqrt_fusion), kind=kOutput, calls=%fused_computation.42 | convolution fusion | flops 4834983936 | bytes 18884096 | tf_op jit(solution)/shard_map/dot_general | solution.py:11
  859.3 21.3 %multiply_convert_fusion.2 = bf16[384,2048]{1,0:T(8,128)(2,1)} fusion(bf16[3072,2048]{1,0:T(8,128)(2,1)} %all-gather.15.cloned.1.call-done, f32[2048]{0:T(1024)S(1)} %copy-done.15, f32[384,3072]{1,0:T(8,128)} %fusion.26, bf16[2048,3072]{1,0:T(8,128)(2,1)} %all-gather.13.cloned.1.call-done, f32[3072]{0:T(1024)S(1)} %dynamic_slice.19, ...), kind=kOutput, calls=%fused_computation.17 | convolution fusion | flops 9677832192 | bytes 33072640 | tf_op jit(solution)/shard_map/dot_general | solution.py:17
  880.6 10.3 %reduce-scatter.8.cloned.1.call-done = bf16[384,1024]{1,0:T(8,128)(2,1)} async-done(((bf16[384,2048]{1,0:T(8,128)(2,1)}), bf16[384,1024]{1,0:T(8,128)(2,1)}) %reduce-scatter.8.cloned.1.call-update) | async-done | bytes 786448 | tf_op jit(solution)/shard_map/reduce_scatter | solution.py:64
  890.9 2.3 fusion.16
  (58 shorter events, 0.4 us)
Async XLA Ops:
  6.5 14.9 %all-gather.27.cloned.1.call-start = ((), (), s32[]{:S(2)}) async-start(), calls=%async_computation.14 | async-start | bytes 2359296 | tf_op jit(solution)/shard_map/all_gather | solution.py:58
  7.3 193.7 %all-gather.11.cloned.1.call-start = ((), (), s32[]{:S(2)}) async-start(), calls=%async_computation.3 | async-start | bytes 14155776 | tf_op jit(solution)/shard_map/all_gather | solution.py:73
  7.3 3.5 copy-start.2
  10.7 366.7 %all-gather.13.cloned.1.call-start = ((), (), s32[]{:S(2)}) async-start(), calls=%async_computation.4 | async-start | bytes 14155776 | tf_op jit(solution)/shard_map/all_gather | solution.py:74
  12.3 541.4 %all-gather.15.cloned.1.call-start = ((), (), s32[]{:S(2)}) async-start(), calls=%async_computation.5 | async-start | bytes 14155776 | tf_op jit(solution)/shard_map/all_gather | solution.py:79
  15.5 0.7 copy-start.10
  15.5 0.8 copy-start.11
  15.5 185.4 %copy-start.12 = (f32[2048]{0:T(1024)S(1)}, f32[2048]{0:T(1024)}, u32[]{:S(2)}) copy-start(f32[2048]{0:T(1024)} %param.19) | copy-start | bytes 24580
  15.5 566.7 %reduce-scatter.4.cloned.1.call-start = ((), (), s32[]{:S(2)}) async-start(), calls=%async_computation.6 | async-start | bytes 2359296 | tf_op jit(solution)/shard_map/reduce_scatter | solution.py:64
  21.4 179.5 %copy-start.5 = (bf16[1,384,2048]{2,1,0:T(8,128)(2,1)S(1)}, bf16[1,384,2048]{2,1,0:T(8,128)(2,1)}, u32[]{:S(2)}) copy-start(bf16[1,384,2048]{2,1,0:T(8,128)(2,1)} %all-gather.27.cloned.1.call-done) | copy-start | bytes 4718596
  23.4 530.3 %copy-start.15 = (f32[2048]{0:T(1024)S(1)}, f32[2048]{0:T(1024)}, u32[]{:S(2)}) copy-start(f32[2048]{0:T(1024)} %param.27) | copy-start | bytes 24580
  575.0 7.3 copy-start.3
  575.0 9.7 %copy-start.7 = (f32[256,1024]{1,0:T(8,128)S(1)}, f32[256,1024]{1,0:T(8,128)}, u32[]{:S(2)}) copy-start(f32[256,1024]{1,0:T(8,128)} %param.28) | copy-start | bytes 3145732
  575.0 20.8 %all-gather.17.cloned.1.call-start = ((), (), s32[]{:S(2)}) async-start(), calls=%async_computation.7 | async-start | bytes 2359296 | tf_op jit(solution)/shard_map/all_gather | solution.py:58
  584.6 1.4 copy-start.8
  584.6 87.4 %all-gather.19.cloned.1.call-start = ((), (), s32[]{:S(2)}) async-start(), calls=%async_computation.8 | async-start | bytes 4718592 | tf_op jit(solution)/shard_map/all_gather | solution.py:89
  585.5 1.4 copy-start.9
  585.6 159.9 %all-gather.21.cloned.1.call-start = ((), (), s32[]{:S(2)}) async-start(), calls=%async_computation.9 | async-start | bytes 4718592 | tf_op jit(solution)/shard_map/all_gather | solution.py:90
  586.9 233.8 %all-gather.23.cloned.1.call-start = ((), (), s32[]{:S(2)}) async-start(), calls=%async_computation.10 | async-start | bytes 4718592 | tf_op jit(solution)/shard_map/all_gather | solution.py:104
  587.8 84.2 %copy-start.13 = (f32[2048]{0:T(1024)S(1)}, f32[2048]{0:T(1024)}, u32[]{:S(2)}) copy-start(f32[2048]{0:T(1024)} %param.20) | copy-start | bytes 24580
  587.8 245.7 %reduce-scatter.6.cloned.1.call-start = ((), (), s32[]{:S(2)}) async-start(), calls=%async_computation.11 | async-start | bytes 2359296 | tf_op jit(solution)/shard_map/reduce_scatter | solution.py:64
  595.8 76.1 %copy-start.4 = (bf16[384,2048]{1,0:T(8,128)(2,1)S(1)}, bf16[384,2048]{1,0:T(8,128)(2,1)}, u32[]{:S(2)}) copy-start(bf16[384,2048]{1,0:T(8,128)(2,1)} %all-gather.17.cloned.1.call-done) | copy-start | bytes 4718596
  597.8 147.7 %dynamic-slice-start = ((f32[2048]{0:T(1024)}, s32[]{:T(128)}), f32[1024]{0:T(1024)S(1)}, s32[]{:S(2)}) async-start(f32[2048]{0:T(1024)} %param.30, s32[]{:T(128)} %select_n.5), calls=%async_computation.15 | async-start | bytes 8704 | tf_op jit(solution)/shard_map/dynamic_slice | solution.py:46
  597.8 147.7 %dynamic-slice-start.1 = ((f32[2048]{0:T(1024)}, s32[]{:T(128)}), f32[1024]{0:T(1024)S(1)}, s32[]{:S(2)}) async-start(f32[2048]{0:T(1024)} %param.31, s32[]{:T(128)} %select_n.5), calls=%async_computation.16 | async-start | bytes 8704 | tf_op jit(solution)/shard_map/dynamic_slice | solution.py:47
  750.4 70.3 %dynamic-slice-start.2 = ((f32[2048]{0:T(1024)}, s32[]{:T(128)}), f32[1024]{0:T(1024)S(1)}, s32[]{:S(2)}) async-start(f32[2048]{0:T(1024)} %param.33, s32[]{:T(128)} %select_n.5), calls=%async_computation.17 | async-start | bytes 8704 | tf_op jit(solution)/shard_map/dynamic_slice | solution.py:48
  750.4 70.3 %copy-start.14 = (f32[2048]{0:T(1024)S(1)}, f32[2048]{0:T(1024)}, u32[]{:S(2)}) copy-start(f32[2048]{0:T(1024)} %param.35) | copy-start | bytes 24580
  826.2 7.3 copy-start
  826.2 20.9 %all-gather.25.cloned.1.call-start = ((), (), s32[]{:S(2)}) async-start(), calls=%async_computation.12 | async-start | bytes 2359296 | tf_op jit(solution)/shard_map/all_gather | solution.py:58
  835.8 13.2 %copy-start.16 = (f32[2048]{0:T(1024)S(1)}, f32[2048]{0:T(1024)}, u32[]{:S(2)}) copy-start(f32[2048]{0:T(1024)} %param.21) | copy-start | bytes 24580
  835.9 55.0 %reduce-scatter.8.cloned.1.call-start = ((), (), s32[]{:S(2)}) async-start(), calls=%async_computation.13 | async-start | bytes 2359296 | tf_op jit(solution)/shard_map/reduce_scatter | solution.py:64
  847.1 1.9 copy-start.6
  880.6 10.3 %copy-start.1 = (bf16[384,1024]{1,0:T(8,128)(2,1)S(1)}, bf16[384,1024]{1,0:T(8,128)(2,1)}, u32[]{:S(2)}) copy-start(bf16[384,1024]{1,0:T(8,128)(2,1)} %add_convert_fusion.1) | copy-start | bytes 2359300
Sparse Core Ops, SparseCore 0:
  8.9 12.5 all-gather.26
  23.6 177.2 all-gather.10
  203.1 174.2 all-gather.12
  379.3 174.2 all-gather.14
  575.1 7.0 reduce-scatter.3
  584.7 11.0 all-gather.16
  598.0 73.9 all-gather.18
  674.1 71.3 all-gather.20
  747.5 73.1 all-gather.22
  826.3 7.1 reduce-scatter.5
  836.0 11.0 all-gather.24
  880.7 10.1 reduce-scatter.7
where the time goes:
time: 901 us; the launch traced here: 900 us
  waiting for transfers between devices  770 us (85%)
  matrix products  78.6 us (9%)
  other arithmetic  30.8 us (3%)
  between operations  13.7 us (2%)
    all_gather x1, waiting for transfers between devices, inner_half(): lax.all_gather(gate_half, 'fs', axis=0, tiled=True)  178 us
    all_gather x1, waiting for transfers between devices, inner_half(): lax.all_gather(down_half, 'fs', axis=1, tiled=True)  176 us
    all_gather x1, waiting for transfers between devices, inner_half(): lax.all_gather(up_half, 'fs', axis=0, tiled=True)  166 us
    all_gather x1, waiting for transfers between devices, on_device(): lax.all_gather(value_half, 'fs', axis=0, tiled=True)  74.2 us
    all_gather x1, waiting for transfers between devices, on_device(): lax.all_gather(mgate_half, 'fs', axis=0, tiled=True)  68.3 us
    all_gather x1, waiting for transfers between devices, on_device(): lax.all_gather(out_half, 'fs', axis=1, tiled=True)  60.6 us
    dot_general x3, matrix products, column_product(): return jnp.dot(left, piece, preferred_element_type=jnp.float32) * scale  48.1 us
    dot_general x3, matrix products, fold_rows(): jnp.dot(normed, pieces[0], preferred_element_type=jnp.float32)  25.9 us
  transfers between devices with their start and end apart: 12, of which 12 were waited for; matrix products, arithmetic and copies ran while one was open for 5% of the time, Pallas kernels for 0%

commit v1 on v0

--- a/solution.py
+++ b/solution.py
@@ -76,7 +76,7 @@
         )
         hidden = (jax.nn.silu(gate * gate_cols) * (upward * up_cols)).astype(jnp.bfloat16)
         terms = column_product(
-            hidden, down_scale, lax.all_gather(down_half, "fs", axis=1, tiled=True)
+            hidden, down_scale, jnp.concatenate(lax.all_gather(down_half, "fs"), axis=1)
         )
         return spread_sum(terms)
 

time: 901 us -> 892 us (0.990)
  waiting for transfers between devices: 770 us -> 753 us
  local copies, waits for them, and re-layouts: 3.84 us -> 20.7 us
  matrix products: 78.6 us -> 69.3 us
    all_gather x1, waiting for transfers between devices: 178 us -> 160 us  [inner_half(): lax.all_gather(gate_half, 'fs', axis=0, tiled=True)]
    reshape x0 -> x1, local copies, waits for them, and re-layouts: none -> 16.7 us  [inner_half(): jnp.concatenate(lax.all_gather(down_half, 'fs'), axis=1)]
    dot_general x3, matrix products: 48.1 us -> 38.7 us  [column_product(): return jnp.dot(left, piece, preferred_element_type=jnp.float32) * scale]
  transfers between devices with their start and end apart: 12 -> 12, of which waited for: 12 -> 12; matrix products, arithmetic and copies ran while one was open for 5% -> 7% of each run, Pallas kernels for 0% -> 0%
where the time goes in v1:
time: 892 us; the launch traced here: 891 us
  waiting for transfers between devices  753 us (84%)
  matrix products  69.3 us (8%)
  other arithmetic  30.6 us (3%)
  local copies, waits for them, and re-layouts  20.7 us (2%)
  between operations  13.7 us (2%)
    all_gather x1, waiting for transfers between devices, inner_half(): lax.all_gather(down_half, 'fs')  178 us
    all_gather x1, waiting for transfers between devices, inner_half(): lax.all_gather(up_half, 'fs', axis=0, tiled=True)  166 us
    all_gather x1, waiting for transfers between devices, inner_half(): lax.all_gather(gate_half, 'fs', axis=0, tiled=True)  160 us
    all_gather x1, waiting for transfers between devices, on_device(): lax.all_gather(value_half, 'fs', axis=0, tiled=True)  74.2 us
    all_gather x1, waiting for transfers between devices, on_device(): lax.all_gather(mgate_half, 'fs', axis=0, tiled=True)  68.3 us
    all_gather x1, waiting for transfers between devices, on_device(): lax.all_gather(out_half, 'fs', axis=1, tiled=True)  60.6 us
    dot_general x3, matrix products, column_product(): return jnp.dot(left, piece, preferred_element_type=jnp.float32) * scale  38.7 us
    dot_general x3, matrix products, fold_rows(): jnp.dot(normed, pieces[0], preferred_element_type=jnp.float32)  25.8 us
  transfers between devices with their start and end apart: 12, of which 12 were waited for; matrix products, arithmetic and copies ran while one was open for 7% of the time, Pallas kernels for 0%

profile of v1, /device:TPU:0, one launch (start us, length us, event | category | flops | bytes accessed | tf_op | source)
XLA Modules:
  0.0 890.9 jit_solution(9603984996028929789)
XLA Ops:
  6.5 0.7 all-gather.26.cloned.1.call-update
  7.3 3.4 convert_element_type.95
  10.7 0.0 all-gather.12.cloned.1.call-start
  10.8 1.4 convert_element_type.92
  12.1 0.0 all-gather.14.cloned.1.call-start
  12.2 3.3 convert_element_type.93
  15.5 0.0 reduce-scatter.4.cloned.1.call-start
  15.5 0.7 copy-done.10
  16.2 5.2 all-gather.26.cloned.1.call-done
  21.4 1.8 fusion.6
  23.2 177.7 %all-gather.28.cloned.1.call-done = bf16[24576,256]{1,0:T(8,128)(2,1)} async-done(((bf16[3072,256]{1,0:T(8,128)(2,1)}), bf16[24576,256]{1,0:T(8,128)(2,1)}) %all-gather.28.cloned.1.call-update) | async-done | bytes 12582928 | tf_op jit(solution)/shard_map/all_gather | solution.py:79
  200.9 16.7 %copy.19 = bf16[3072,8,256]{0,2,1:T(8,128)(2,1)} copy(bf16[3072,8,256]{2,0,1:T(8,128)(2,1)} %bitcast.58) | data formatting | bytes 25165824 | tf_op jit(solution)/shard_map/reshape | solution.py:79
  217.6 159.8 %all-gather.12.cloned.1.call-done = bf16[2048,3072]{1,0:T(8,128)(2,1)} async-done(((bf16[256,3072]{1,0:T(8,128)(2,1)}), bf16[2048,3072]{1,0:T(8,128)(2,1)}) %all-gather.12.cloned.1.call-update) | async-done | bytes 12582928 | tf_op jit(solution)/shard_map/all_gather | solution.py:73
  377.4 10.3 %fusion.22 = f32[384,3072]{1,0:T(8,128)} fusion(bf16[2048,3072]{1,0:T(8,128)(2,1)} %all-gather.12.cloned.1.call-done, bf16[1,384,2048]{2,1,0:T(8,128)(2,1)S(1)} %copy-done.5, f32[2048]{0:T(1024)S(1)} %copy-done.12, f32[384]{0:T(512)S(1)} %add_rsqrt_fusion.3), kind=kOutput, calls=%fused_computation.41 | convolution fusion | flops 4834983936 | bytes 18884096 | tf_op jit(solution)/shard_map/dot_general | solution.py:11
  387.8 166.0 %all-gather.14.cloned.1.call-done = bf16[2048,3072]{1,0:T(8,128)(2,1)} async-done(((bf16[256,3072]{1,0:T(8,128)(2,1)}), bf16[2048,3072]{1,0:T(8,128)(2,1)}) %all-gather.14.cloned.1.call-update) | async-done | bytes 12582928 | tf_op jit(solution)/shard_map/all_gather | solution.py:74
  553.8 16.6 %multiply_convert_fusion.4 = bf16[384,2048]{1,0:T(8,128)(2,1)} fusion(bf16[3072,2048]{0,1:T(8,128)(2,1)} %bitcast.56, f32[2048]{0:T(1024)S(1)} %copy-done.15, f32[384,3072]{1,0:T(8,128)} %fusion.22, bf16[2048,3072]{1,0:T(8,128)(2,1)} %all-gather.14.cloned.1.call-done, f32[3072]{0:T(1024)S(1)} %dynamic_slice.19, f32[3072]{0:T(1024)S(1)} %dynamic_slice.18, ...), kind=kOutput, calls=%fused_computation.19 | convolution fusion | flops 9677832192 | bytes 33072640 | tf_op jit(solution)/shard_map/dot_general | solution.py:17
  570.5 0.0 all-gather.16.cloned.1.call-start
  570.5 7.2 reduce-scatter.4.cloned.1.call-done
  577.7 2.3 fusion.9
  580.1 0.9 convert_element_type.102
  581.1 0.4 copy-done.8
  581.5 0.9 convert_element_type.103
  582.3 0.0 all-gather.22.cloned.1.call-start
  582.4 0.9 convert_element_type.107
  583.3 0.2 reduce-scatter.6.cloned.1.call-start
  583.5 1.3 fusion.34
  584.8 1.6 constant_dynamic-slice_fusion
  586.4 4.9 all-gather.16.cloned.1.call-done
  591.3 1.9 fusion
  593.2 74.2 %all-gather.18.cloned.1.call-done = bf16[2048,1024]{1,0:T(8,128)(2,1)} async-done(((bf16[256,1024]{1,0:T(8,128)(2,1)}), bf16[2048,1024]{1,0:T(8,128)(2,1)}) %all-gather.18.cloned.1.call-update) | async-done | bytes 4194320 | tf_op jit(solution)/shard_map/all_gather | solution.py:89
  667.4 5.2 fusion.29
  672.6 68.3 %all-gather.20.cloned.1.call-done = bf16[2048,1024]{1,0:T(8,128)(2,1)} async-done(((bf16[256,1024]{1,0:T(8,128)(2,1)}), bf16[2048,1024]{1,0:T(8,128)(2,1)}) %all-gather.20.cloned.1.call-update) | async-done | bytes 4194320 | tf_op jit(solution)/shard_map/all_gather | solution.py:90
  740.9 4.7 multiply_convert_fusion.6
  745.6 0.2 convert_element_type.105
  745.9 7.3 multiply_reduce_fusion
  753.1 2.5 psum.7
  755.6 60.6 %all-gather.22.cloned.1.call-done = bf16[1024,2048]{1,0:T(8,128)(2,1)} async-done(((bf16[1024,256]{1,0:T(8,128)(2,1)}), bf16[1024,2048]{1,0:T(8,128)(2,1)}) %all-gather.22.cloned.1.call-update) | async-done | bytes 4194320 | tf_op jit(solution)/shard_map/all_gather | solution.py:104
  816.2 5.5 multiply_convert_fusion.3
  821.7 0.0 all-gather.24.cloned.1.call-start
  821.7 7.2 reduce-scatter.6.cloned.1.call-done
  829.0 2.3 add_convert_fusion.1
  831.3 0.3 reduce-scatter.8.cloned.1.call-start
  831.6 11.0 %all-gather.24.cloned.1.call-done = bf16[384,2048]{1,0:T(8,128)(2,1)} async-done(((bf16[384,1024]{1,0:T(8,128)(2,1)}), bf16[384,2048]{1,0:T(8,128)(2,1)}) %all-gather.24.cloned.1.call-update) | async-done | bytes 1572880 | tf_op jit(solution)/shard_map/all_gather | solution.py:58
  842.5 1.9 fusion.3
  844.5 10.3 %fusion.26 = f32[384,3072]{1,0:T(8,128)} fusion(bf16[2048,3072]{1,0:T(8,128)(2,1)} %all-gather.12.cloned.1.call-done, bf16[384,2048]{1,0:T(8,128)(2,1)S(1)} %copy-done.6, f32[2048]{0:T(1024)S(1)} %copy-done.16, f32[384]{0:T(512)S(1)} %add_rsqrt_fusion), kind=kOutput, calls=%fused_computation.42 | convolution fusion | flops 4834983936 | bytes 18884096 | tf_op jit(solution)/shard_map/dot_general | solution.py:11
  854.8 16.6 %multiply_convert_fusion.2 = bf16[384,2048]{1,0:T(8,128)(2,1)} fusion(bf16[3072,2048]{0,1:T(8,128)(2,1)} %bitcast.57, f32[2048]{0:T(1024)S(1)} %copy-done.15, f32[384,3072]{1,0:T(8,128)} %fusion.26, bf16[2048,3072]{1,0:T(8,128)(2,1)} %all-gather.14.cloned.1.call-done, f32[3072]{0:T(1024)S(1)} %dynamic_slice.19, f32[3072]{0:T(1024)S(1)} %dynamic_slice.18, ...), kind=kOutput, calls=%fused_computation.17 | convolution fusion | flops 9677832192 | bytes 33072640 | tf_op jit(solution)/shard_map/dot_general | solution.py:17
  871.4 10.3 %reduce-scatter.8.cloned.1.call-done = bf16[384,1024]{1,0:T(8,128)(2,1)} async-done(((bf16[384,2048]{1,0:T(8,128)(2,1)}), bf16[384,1024]{1,0:T(8,128)(2,1)}) %reduce-scatter.8.cloned.1.call-update) | async-done | bytes 786448 | tf_op jit(solution)/shard_map/reduce_scatter | solution.py:64
  881.7 2.3 fusion.16
  (59 shorter events, 0.4 us)
Async XLA Ops:
  6.5 14.9 %all-gather.26.cloned.1.call-start = ((), (), s32[]{:S(2)}) async-start(), calls=%async_computation.13 | async-start | bytes 2359296 | tf_op jit(solution)/shard_map/all_gather | solution.py:58
  7.3 193.7 %all-gather.28.cloned.1.call-start = ((), (), s32[]{:S(2)}) async-start(), calls=%async_computation.14 | async-start | bytes 14155776 | tf_op jit(solution)/shard_map/all_gather | solution.py:79
  7.3 3.5 copy-start.2
  10.7 366.7 %all-gather.12.cloned.1.call-start = ((), (), s32[]{:S(2)}) async-start(), calls=%async_computation.3 | async-start | bytes 14155776 | tf_op jit(solution)/shard_map/all_gather | solution.py:73
  12.1 541.7 %all-gather.14.cloned.1.call-start = ((), (), s32[]{:S(2)}) async-start(), calls=%async_computation.4 | async-start | bytes 14155776 | tf_op jit(solution)/shard_map/all_gather | solution.py:74
  15.5 0.7 copy-start.10
  15.5 0.8 copy-start.11
  15.5 562.2 %reduce-scatter.4.cloned.1.call-start = ((), (), s32[]{:S(2)}) async-start(), calls=%async_computation.5 | async-start | bytes 2359296 | tf_op jit(solution)/shard_map/reduce_scatter | solution.py:64
  200.9 176.5 %copy-start.5 = (bf16[1,384,2048]{2,1,0:T(8,128)(2,1)S(1)}, bf16[1,384,2048]{2,1,0:T(8,128)(2,1)}, u32[]{:S(2)}) copy-start(bf16[1,384,2048]{2,1,0:T(8,128)(2,1)} %all-gather.26.cloned.1.call-done) | copy-start | bytes 4718596
  200.9 176.5 %copy-start.12 = (f32[2048]{0:T(1024)S(1)}, f32[2048]{0:T(1024)}, u32[]{:S(2)}) copy-start(f32[2048]{0:T(1024)} %param.19) | copy-start | bytes 24580
  217.6 336.2 %copy-start.15 = (f32[2048]{0:T(1024)S(1)}, f32[2048]{0:T(1024)}, u32[]{:S(2)}) copy-start(f32[2048]{0:T(1024)} %param.27) | copy-start | bytes 24580
  570.4 7.3 copy-start.3
  570.4 9.7 %copy-start.7 = (f32[256,1024]{1,0:T(8,128)S(1)}, f32[256,1024]{1,0:T(8,128)}, u32[]{:S(2)}) copy-start(f32[256,1024]{1,0:T(8,128)} %param.28) | copy-start | bytes 3145732
  570.5 20.8 %all-gather.16.cloned.1.call-start = ((), (), s32[]{:S(2)}) async-start(), calls=%async_computation.6 | async-start | bytes 2359296 | tf_op jit(solution)/shard_map/all_gather | solution.py:58
  580.0 1.4 copy-start.8
  580.1 87.4 %all-gather.18.cloned.1.call-start = ((), (), s32[]{:S(2)}) async-start(), calls=%async_computation.7 | async-start | bytes 4718592 | tf_op jit(solution)/shard_map/all_gather | solution.py:89
  581.0 1.4 copy-start.9
  581.0 159.9 %all-gather.20.cloned.1.call-start = ((), (), s32[]{:S(2)}) async-start(), calls=%async_computation.8 | async-start | bytes 4718592 | tf_op jit(solution)/shard_map/all_gather | solution.py:90
  582.3 233.8 %all-gather.22.cloned.1.call-start = ((), (), s32[]{:S(2)}) async-start(), calls=%async_computation.9 | async-start | bytes 4718592 | tf_op jit(solution)/shard_map/all_gather | solution.py:104
  583.3 84.2 %copy-start.13 = (f32[2048]{0:T(1024)S(1)}, f32[2048]{0:T(1024)}, u32[]{:S(2)}) copy-start(f32[2048]{0:T(1024)} %param.20) | copy-start | bytes 24580
  583.3 245.7 %reduce-scatter.6.cloned.1.call-start = ((), (), s32[]{:S(2)}) async-start(), calls=%async_computation.10 | async-start | bytes 2359296 | tf_op jit(solution)/shard_map/reduce_scatter | solution.py:64
  591.3 76.1 %copy-start.4 = (bf16[384,2048]{1,0:T(8,128)(2,1)S(1)}, bf16[384,2048]{1,0:T(8,128)(2,1)}, u32[]{:S(2)}) copy-start(bf16[384,2048]{1,0:T(8,128)(2,1)} %all-gather.16.cloned.1.call-done) | copy-start | bytes 4718596
  593.2 147.7 %dynamic-slice-start = ((f32[2048]{0:T(1024)}, s32[]{:T(128)}), f32[1024]{0:T(1024)S(1)}, s32[]{:S(2)}) async-start(f32[2048]{0:T(1024)} %param.30, s32[]{:T(128)} %select_n.5), calls=%async_computation.15 | async-start | bytes 8704 | tf_op jit(solution)/shard_map/dynamic_slice | solution.py:46
  593.2 147.7 %dynamic-slice-start.1 = ((f32[2048]{0:T(1024)}, s32[]{:T(128)}), f32[1024]{0:T(1024)S(1)}, s32[]{:S(2)}) async-start(f32[2048]{0:T(1024)} %param.31, s32[]{:T(128)} %select_n.5), calls=%async_computation.16 | async-start | bytes 8704 | tf_op jit(solution)/shard_map/dynamic_slice | solution.py:47
  745.8 70.3 %dynamic-slice-start.2 = ((f32[2048]{0:T(1024)}, s32[]{:T(128)}), f32[1024]{0:T(1024)S(1)}, s32[]{:S(2)}) async-start(f32[2048]{0:T(1024)} %param.33, s32[]{:T(128)} %select_n.5), calls=%async_computation.17 | async-start | bytes 8704 | tf_op jit(solution)/shard_map/dynamic_slice | solution.py:48
  745.8 70.3 %copy-start.14 = (f32[2048]{0:T(1024)S(1)}, f32[2048]{0:T(1024)}, u32[]{:S(2)}) copy-start(f32[2048]{0:T(1024)} %param.35) | copy-start | bytes 24580
  821.7 7.3 copy-start
  821.7 20.9 %all-gather.24.cloned.1.call-start = ((), (), s32[]{:S(2)}) async-start(), calls=%async_computation.11 | async-start | bytes 2359296 | tf_op jit(solution)/shard_map/all_gather | solution.py:58
  831.3 13.2 %copy-start.16 = (f32[2048]{0:T(1024)S(1)}, f32[2048]{0:T(1024)}, u32[]{:S(2)}) copy-start(f32[2048]{0:T(1024)} %param.21) | copy-start | bytes 24580
  831.3 50.4 %reduce-scatter.8.cloned.1.call-start = ((), (), s32[]{:S(2)}) async-start(), calls=%async_computation.12 | async-start | bytes 2359296 | tf_op jit(solution)/shard_map/reduce_scatter | solution.py:64
  842.5 1.9 copy-start.6
  871.4 10.3 %copy-start.1 = (bf16[384,1024]{1,0:T(8,128)(2,1)S(1)}, bf16[384,1024]{1,0:T(8,128)(2,1)}, u32[]{:S(2)}) copy-start(bf16[384,1024]{1,0:T(8,128)(2,1)} %add_convert_fusion.1) | copy-start | bytes 2359300
Sparse Core Ops, SparseCore 0:
  8.9 12.5 all-gather.25
  23.6 177.2 all-gather.27
  203.1 174.2 all-gather.11
  379.5 174.2 all-gather.13
  570.6 7.1 reduce-scatter.3
  580.2 11.0 all-gather.15
  593.4 73.9 all-gather.17
  669.5 71.3 all-gather.19
  743.0 73.1 all-gather.21
  821.8 7.1 reduce-scatter.5
  831.4 11.0 all-gather.23
  871.5 10.1 reduce-scatter.7
